TPU v7x, 32 devices: a whole 2x2x4 slice. The times are simulated.
32 devices in a mesh: ep: 8 (over z, y), tp: 4 (over x, core).
Axes of the slice: x: 2, y: 2, z: 4, core: 2. Of those that a mesh axis runs over, the one named last changes fastest.
Arguments:
- hidden_in: bfloat16 [384, 2048], P('ep'), may hold values from -6 to 6
- carried_state: float32 [384, 4, 128, 256], P('ep', 'tp'), may hold values from -6 to 6
- input_gain: bfloat16 [2048], replicated, may hold values from 0.099609375 to 1.8984375
- query_weight: bfloat16 [2048, 512], P(None, 'tp'), may hold values from -0.125 to 0.125
- key_weight: bfloat16 [2048, 512], P(None, 'tp'), may hold values from -0.125 to 0.125
- value_weight: bfloat16 [2048, 1024], P(None, 'tp'), may hold values from -0.125 to 0.125
- outgate_weight: bfloat16 [2048, 1024], P(None, 'tp'), may hold values from -0.125 to 0.125
- decay_weight: bfloat16 [2048, 512], P(None, 'tp'), may hold values from -0.5 to 0.5
- decay_shift: float32 [384, 512], P('ep', 'tp'), may hold values from -0.7 to 0
- head_gain: bfloat16 [4, 256], P('tp'), may hold values from 0.099609375 to 1.8984375
- output_weight: bfloat16 [1024, 2048], P('tp'), may hold values from -0.1875 to 0.1875
- channel_gain: bfloat16 [2048], replicated, may hold values from 0.099609375 to 1.8984375
- branch_gate: bfloat16 [2048], replicated, may hold values from -0.125 to 0.125
- routes: int32 [384, 2], P('ep'), may hold values from 0 to 7, all different within a row; in each aligned block of 48 rows (0 to 47, 48 to 95, ...) at most 14 rows name the same one
- route_weights: float32 [384, 2], P('ep'), may hold values from 0.1 to 1
- expert_gate: bfloat16 [8, 2048, 3072], P('ep', None, 'tp'), may hold values from -0.125 to 0.125
- expert_up: bfloat16 [8, 2048, 3072], P('ep', None, 'tp'), may hold values from -0.125 to 0.125
- expert_down: bfloat16 [8, 3072, 2048], P('ep', 'tp'), may hold values from -0.109375 to 0.109375
- dense_gate: bfloat16 [2048, 4096], P('tp', 'ep'), may hold values from -0.125 to 0.125
- dense_up: bfloat16 [2048, 4096], P('tp', 'ep'), may hold values from -0.125 to 0.125
- dense_down: bfloat16 [4096, 2048], P('ep', 'tp'), may hold values from -0.09375 to 0.09375
Outputs:
- mixed: bfloat16 [384, 2048], P('ep', 'tp')
- new_state: float32 [384, 4, 128, 256], P('ep', 'tp')
Inputs may be any that keep to these rules, and one draw needn't show every extreme that they name: `routes`: each row names 2 different experts. Among the rows of one index of ep no expert is named more than 14 times, and in every draw some expert is named exactly 14 times by the rows of some index.
All inputs are finite; a program needn't handle non-finite values.
Results may differ from a plain program's by a relative error of at most 0.02.
Values may be sent and summed in bfloat16 or wider, within the bound.
A program may use at most 128 MiB of HBM per device.

v0:
```python
import jax
import jax.numpy as jnp
from jax import lax
from jax.sharding import PartitionSpec as P

EPSILON = 1e-06
TAU_DECAY = 16.0


def rms_factor(values):
    return lax.rsqrt(jnp.mean(values * values, axis=-1, keepdims=True) + EPSILON)


def rounded(values):
    return lax.optimization_barrier(values.astype(jnp.bfloat16)).astype(jnp.float32)


def matmul(left, right):
    return jnp.dot(left, right, preferred_element_type=jnp.float32)


def unit_totals(paired):
    return lax.psum(paired.astype(jnp.bfloat16), "tp").astype(jnp.float32)


def body(
    hidden_in,
    carried_state,
    input_gain,
    query_weight,
    key_weight,
    value_weight,
    outgate_weight,
    decay_weight,
    decay_shift,
    head_gain,
    output_weight,
    channel_gain,
    branch_gate,
    routes,
    route_weights,
    expert_gate,
    expert_up,
    expert_down,
    dense_gate,
    dense_up,
    dense_down,
):
    tokens_here, width = hidden_in.shape
    heads_here, key_dim, value_dim = carried_state.shape[1:]
    quarter = width // lax.axis_size("tp")
    lane_start = lax.axis_index("tp") * quarter
    inputs = hidden_in.astype(jnp.float32)
    normed = (inputs * rms_factor(inputs) * input_gain.astype(jnp.float32)).astype(jnp.bfloat16)
    query = matmul(normed, query_weight).astype(jnp.bfloat16)
    key_rows = matmul(normed, key_weight).astype(jnp.bfloat16)
    value_rows = matmul(normed, value_weight).astype(jnp.bfloat16)
    outgate = matmul(normed, outgate_weight).astype(jnp.bfloat16)
    decay = jnp.exp(jax.nn.log_sigmoid(matmul(normed, decay_weight)) / TAU_DECAY + decay_shift)
    decay = decay.reshape(tokens_here, heads_here, key_dim)
    query_scaled = query.astype(jnp.float32).reshape(
        tokens_here, heads_here, key_dim
    ) * key_dim ** (-0.5)
    key_vals = key_rows.astype(jnp.float32).reshape(tokens_here, heads_here, key_dim)
    value_vals = value_rows.astype(jnp.float32).reshape(tokens_here, heads_here, value_dim)
    new_state = decay[..., None] * carried_state + key_vals[..., None] * value_vals[:, :, None, :]
    readout = jnp.einsum("bhk,bhkv->bhv", query_scaled, new_state, precision=lax.Precision.HIGHEST)
    gate_vals = jax.nn.silu(outgate.astype(jnp.float32).reshape(tokens_here, heads_here, value_dim))
    gated = (readout * rms_factor(readout) * head_gain.astype(jnp.float32) * gate_vals).astype(
        jnp.bfloat16
    )
    partial_out = rounded(matmul(gated.reshape(tokens_here, heads_here * value_dim), output_weight))
    own_gain = lax.dynamic_slice_in_dim(channel_gain.astype(jnp.float32), lane_start, quarter, 0)
    own_branch = lax.dynamic_slice_in_dim(branch_gate.astype(jnp.float32), lane_start, quarter, 0)
    attended_own = lax.psum_scatter(
        partial_out.astype(jnp.bfloat16), "tp", scatter_dimension=1, tiled=True
    ).astype(jnp.float32)
    middle_own = rounded(lax.dynamic_slice_in_dim(inputs, lane_start, quarter, 1) + attended_own)
    total_squares, gate_inner = lax.psum(
        (
            jnp.sum(middle_own * middle_own, axis=-1),
            jnp.sum(middle_own * own_gain * own_branch, axis=-1),
        ),
        "tp",
    )
    factor = lax.rsqrt(total_squares / width + EPSILON)
    branch = jax.nn.sigmoid(gate_inner * factor)
    ffn_own = (middle_own * factor[:, None] * own_gain).astype(jnp.bfloat16)
    expert_count = lax.axis_size("ep")
    topk = routes.shape[1]
    capacity = tokens_here * topk // expert_count + 2
    chosen = (
        routes[:, :, None] == jnp.arange(expert_count, dtype=jnp.int32)[None, None, :]
    ).astype(jnp.int32)
    chosen_flat = chosen.reshape(tokens_here * topk, expert_count)
    earlier = jnp.cumsum(chosen_flat, axis=0) - chosen_flat
    slot_index = jnp.sum(earlier * chosen_flat, axis=1).reshape(tokens_here, topk)
    position = routes * capacity + slot_index
    slot_table = jnp.arange(expert_count * capacity, dtype=jnp.int32)
    selector = jnp.sum(
        (slot_table[:, None, None] == position[None, :, :]).astype(jnp.bfloat16), axis=2
    )
    send_width = ffn_own.shape[1]
    outgoing = (
        matmul(selector, ffn_own).astype(jnp.bfloat16).reshape(expert_count, capacity, send_width)
    )
    full_rows = lax.all_gather(
        lax.all_to_all(outgoing, "ep", split_axis=0, concat_axis=0, tiled=True),
        "tp",
        axis=2,
        tiled=True,
    )
    sources = full_rows.shape[0]
    items = full_rows.shape[1]
    flat_rows = full_rows.reshape(sources * items, width)
    gate_part = matmul(flat_rows, expert_gate[0])
    up_part = matmul(flat_rows, expert_up[0])
    hidden = (jax.nn.silu(gate_part) * up_part).astype(jnp.bfloat16)
    block_out = rounded(matmul(hidden, expert_down[0]))
    summed = lax.psum_scatter(
        block_out.astype(jnp.bfloat16), "tp", scatter_dimension=1, tiled=True
    ).astype(jnp.float32)
    returned = lax.all_to_all(
        summed.reshape(sources, items, quarter).astype(jnp.bfloat16),
        "ep",
        split_axis=0,
        concat_axis=0,
        tiled=True,
    ).astype(jnp.float32)
    flat_back = returned.reshape(expert_count * capacity, quarter)
    picked = jnp.take(flat_back, position.reshape(-1), axis=0).reshape(tokens_here, topk, quarter)
    routed_own = jnp.sum(picked * route_weights[:, :, None], axis=1)
    piece = lax.all_gather(ffn_own, "ep", axis=0, tiled=True)
    paired = unit_totals(
        jnp.concatenate([matmul(piece, dense_gate), matmul(piece, dense_up)], axis=1)
    )
    units = dense_gate.shape[1]
    dense_hidden = (jax.nn.silu(paired[:, :units]) * paired[:, units:]).astype(jnp.bfloat16)
    dense_own = lax.psum_scatter(
        matmul(dense_hidden, dense_down).astype(jnp.bfloat16), "ep", scatter_dimension=0, tiled=True
    ).astype(jnp.float32)
    mixed = (middle_own + branch[:, None] * dense_own + routed_own).astype(jnp.bfloat16)
    return (mixed, new_state)


def solution(mesh):
    in_specs = (
        P("ep", None),
        P("ep", "tp", None, None),
        P(),
        P(None, "tp"),
        P(None, "tp"),
        P(None, "tp"),
        P(None, "tp"),
        P(None, "tp"),
        P("ep", "tp"),
        P("tp", None),
        P("tp", None),
        P(),
        P(),
        P("ep", None),
        P("ep", None),
        P("ep", None, "tp"),
        P("ep", None, "tp"),
        P("ep", "tp", None),
        P("tp", "ep"),
        P("tp", "ep"),
        P("ep", "tp"),
    )
    out_specs = (P("ep", "tp"), P("ep", "tp", None, None))
    return jax.shard_map(body, mesh=mesh, in_specs=in_specs, out_specs=out_specs, check_vma=False)
```

profile of v0, /device:TPU:1, one launch (start us, length us, event | category | flops | bytes accessed | tf_op | source)
XLA Modules:
  0.0 229.6 jit_solution(6923637545601130041)
XLA Ops:
  7.2 0.0 reduce-scatter.4.cloned.1.call-start
  7.2 0.8 convert_element_type.104
  8.1 1.1 multiply_reduce_fusion
  9.2 1.7 fusion.18
  10.9 1.4 fusion.19
  12.3 1.4 fusion.21
  13.7 1.4 fusion.50
  15.1 4.5 %multiply_add_fusion = f32[48,1,128,256]{3,2,1,0:T(8,128)S(1)} fusion(f32[48,1,128,256]{3,2,1,0:T(8,128)} %param.22, f32[48,256]{1,0:T(8,128)S(1)} %fusion.18, f32[48,128]{1,0:T(8,128)S(1)} %fusion.19, f32[48,128]{1,0:T(8,128)S(1)} %fusion.50), kind=kLoop, calls=%fused_computation.3 | loop fusion | flops 4718592 | bytes 12681216 | tf_op jit(solution)/shard_map/add | solution.py:66
  19.7 3.1 %fusion = f32[48,1,256]{2,1,0:T(1,128)S(1)} fusion(f32[48,128,1]{1,2,0:T(1,128)S(1)} %bitcast.55, f32[48,1,128,256]{3,2,1,0:T(8,128)S(1)} %multiply_add_fusion), kind=kOutput, calls=%fused_computation.1 | convolution fusion | flops 18874368 | bytes 6365184 | tf_op jit(solution)/shard_map/bhk,bhkv->bhv/dot_general | solution.py:67
  22.7 0.1 fusion.39
  22.9 3.0 %convolution_convert_fusion = bf16[48,2048]{1,0:T(8,128)(2,1)} fusion(bf16[256,2048]{1,0:T(8,128)(2,1)} %param.31, bf16[2048,256]{1,0:T(8,128)(2,1)} %param.27, f32[48,1,256]{2,1,0:T(1,128)S(1)} %fusion, f32[256]{0:T(256)S(1)} %bitcast.56, f32[48]{0:T(128)S(1)} %add_rsqrt_fusion.1, f32[2048]{0:T(1024)S(1)} %convert_element_type.104, ...), kind=kOutput, calls=%fused_computation.11 | convolution fusion | flops 101277696 | bytes 2549120 | tf_op jit(solution)/shard_map/dot_general | solution.py:19
  25.9 0.0 reduce-scatter.4.cloned.1.call-update
  26.0 0.1 copy.36
  26.0 0.1 eq.29
  26.2 0.1 fusion.43
  26.3 0.1 reduce_window_sum.11
  26.4 0.2 select_reduce_fusion
  26.6 0.8 dynamic-slice_convert_fusion
  27.4 0.8 convert_element_type.103
  28.1 0.1 reshape.135
  28.2 0.1 copy.37
  28.3 0.5 compare_and_fusion
  28.9 0.1 fusion.46
  29.0 18.7 %reduce-scatter.4.cloned.1.call-done = bf16[48,512]{1,0:T(8,128)(2,1)} async-done(((bf16[48,2048]{1,0:T(8,128)(2,1)}), bf16[48,512]{1,0:T(8,128)(2,1)}) %reduce-scatter.4.cloned.1.call-update) | async-done | bytes 49168 | tf_op jit(solution)/shard_map/reduce_scatter | solution.py:75
  47.6 0.9 add_convert_fusion
  48.6 0.1 fusion.33
  48.7 6.0 %all-reduce = (f32[48]{0:T(128)S(1)}, f32[48]{0:T(128)S(1)}) all-reduce(f32[48]{0:T(128)S(1)} %get-tuple-element.3, f32[48]{0:T(128)S(1)} %get-tuple-element.2), channel_id=1, replica_groups=mesh['ep'=8,'tp'=4] {'tp'}, use_global_device_ids=true, to_apply=%region_6.7 | all-reduce | flops 96 | bytes 768 | tf_op jit(solution)/shard_map/psum | solution.py:79
  54.7 0.6 add_divide_fusion
  55.3 0.1 fusion.36
  55.4 25.2 %all_gather.6 = bf16[384,512]{1,0:T(8,128)(2,1)S(1)} all-gather(bf16[48,512]{1,0:T(8,128)(2,1)S(1)} %fusion.36), channel_id=1, replica_groups=mesh['ep'=8,'tp'=4] {'ep'}, dimensions={0}, use_global_device_ids=true | all-gather | bytes 442368 | tf_op jit(solution)/shard_map/all_gather | solution.py:133
  80.6 0.8 convolution_convert_fusion.4
  81.4 1.6 reshape.136
  83.0 5.2 %all-to-all-start = ((bf16[8,14,512]{2,1,0:T(8,128)(2,1)}), bf16[8,14,512]{2,1,0:T(8,128)(2,1)}, u32[]{:S(2)}, u32[]{:S(2)}) async-start(bf16[8,14,512]{2,1,0:T(8,128)(2,1)} %reshape.136), calls=%async_computation.2 | async-start | bytes 262144 | tf_op jit(solution)/shard_map/all_to_all | solution.py:108
  88.2 0.0 all-reduce.3.cloned.1.call-start
  88.2 1.4 convolution_convert_fusion.2
  89.6 1.4 convolution_convert_fusion.3
  91.0 1.0 pad_maximum_fusion
  92.1 0.0 all-reduce.3.cloned.1.call-update
  92.1 0.0 reduce-scatter.8.cloned.1.call-start
  92.1 2.3 %all-to-all-done = bf16[8,14,512]{2,1,0:T(8,128)(2,1)} async-done(((bf16[8,14,512]{2,1,0:T(8,128)(2,1)}), bf16[8,14,512]{2,1,0:T(8,128)(2,1)}, u32[]{:S(2)}, u32[]{:S(2)}) %all-to-all-start) | async-done | bytes 114720 | tf_op jit(solution)/shard_map/all_to_all | solution.py:108
  94.5 18.2 %all_gather.7 = bf16[8,14,2048]{2,1,0:T(8,128)(2,1)} all-gather(bf16[8,14,512]{2,1,0:T(8,128)(2,1)} %all-to-all-done), channel_id=1, replica_groups=mesh['ep'=8,'tp'=4] {'tp'}, dimensions={2}, use_global_device_ids=true | all-gather | bytes 573440 | tf_op jit(solution)/shard_map/all_gather | solution.py:107
  112.6 1.9 reshape.137
  114.6 2.6 %fusion.6 = f32[112,768]{1,0:T(8,128)S(1)} fusion(bf16[112,2048]{1,0:T(8,128)(2,1)} %reshape.137, bf16[1,2048,768]{2,1,0:T(8,128)(2,1)} %param.36), kind=kOutput, calls=%fused_computation.8 | convolution fusion | flops 352321536 | bytes 3948544 | tf_op jit(solution)/shard_map/dot_general | solution.py:19
  117.2 4.1 %fusion.8 = bf16[112,2048]{1,0:T(8,128)(2,1)} fusion(bf16[1,768,2048]{2,1,0:T(8,128)(2,1)S(1)} %copy-done, bf16[112,2048]{1,0:T(8,128)(2,1)} %reshape.137, bf16[1,2048,768]{2,1,0:T(8,128)(2,1)} %param.37, f32[112,768]{1,0:T(8,128)S(1)} %fusion.6), kind=kOutput, calls=%fused_computation.10 | convolution fusion | flops 705388544 | bytes 7553024 | tf_op jit(solution)/shard_map/dot_general | solution.py:19
  121.3 0.0 reduce-scatter.8.cloned.1.call-update
  121.3 0.0 reduce-scatter.6.cloned.1.call-start
  121.4 11.5 %all-reduce.3.cloned.1.call-done = bf16[384,1024]{1,0:T(8,128)(2,1)} async-done(((bf16[384,1024]{1,0:T(8,128)(2,1)}), bf16[384,1024]{1,0:T(8,128)(2,1)}) %all-reduce.3.cloned.1.call-update) | async-done | bytes 786448 | tf_op jit(solution)/shard_map/psum | solution.py:23
  132.8 1.3 convert_element_type.122
  134.2 2.2 convolution_convert_fusion.1
  136.4 0.0 reduce-scatter.6.cloned.1.call-update
  136.4 0.1 copy.39
  136.5 0.1 reshape.140
  136.6 21.4 %reduce-scatter.8.cloned.1.call-done = bf16[112,512]{1,0:T(8,128)(2,1)} async-done(((bf16[112,2048]{1,0:T(8,128)(2,1)}), bf16[112,512]{1,0:T(8,128)(2,1)}) %reduce-scatter.8.cloned.1.call-update) | async-done | bytes 114704 | tf_op jit(solution)/shard_map/reduce_scatter | solution.py:120
  158.0 1.6 convert_element_type.131
  159.6 5.2 %all-to-all-start.1 = ((bf16[8,14,512]{2,1,0:T(8,128)(2,1)}), bf16[8,14,512]{2,1,0:T(8,128)(2,1)S(1)}, u32[]{:S(2)}, u32[]{:S(2)}) async-start(bf16[8,14,512]{2,1,0:T(8,128)(2,1)} %convert_element_type.131), calls=%async_computation.4 | async-start | bytes 262144 | tf_op jit(solution)/shard_map/all_to_all | solution.py:123
  164.8 0.7 copy.38
  165.5 0.7 copy.40
  166.2 0.6 pad_clamp_fusion
  166.8 4.3 %all-to-all-done.1 = bf16[8,14,512]{2,1,0:T(8,128)(2,1)S(1)} async-done(((bf16[8,14,512]{2,1,0:T(8,128)(2,1)}), bf16[8,14,512]{2,1,0:T(8,128)(2,1)S(1)}, u32[]{:S(2)}, u32[]{:S(2)}) %all-to-all-start.1) | async-done | bytes 114720 | tf_op jit(solution)/shard_map/all_to_all | solution.py:123
  171.2 1.5 gather_fusion
  172.6 1.0 gather.7
  173.7 1.1 multiply_reduce_fusion.1
  174.8 46.8 %reduce-scatter.6.cloned.1.call-done = bf16[48,512]{1,0:T(8,128)(2,1)} async-done(((bf16[384,512]{1,0:T(8,128)(2,1)}), bf16[48,512]{1,0:T(8,128)(2,1)}) %reduce-scatter.6.cloned.1.call-update) | async-done | bytes 49168 | tf_op jit(solution)/shard_map/reduce_scatter | solution.py:139
  221.6 1.5 fusion.38
  (23 shorter events, 0.1 us)
Async XLA Ops:
  7.2 110.0 %copy-start = (bf16[1,768,2048]{2,1,0:T(8,128)(2,1)S(1)}, bf16[1,768,2048]{2,1,0:T(8,128)(2,1)}, u32[]{:S(2)}) copy-start(bf16[1,768,2048]{2,1,0:T(8,128)(2,1)} %param.38) | copy-start | bytes 9437188
  7.2 40.5 %reduce-scatter.4.cloned.1.call-start = ((), (), s32[]{:S(2)}) async-start(), calls=%async_computation.5 | async-start | bytes 245760 | tf_op jit(solution)/shard_map/reduce_scatter | solution.py:75
  19.6 3.1 %copy-start.1 = (f32[48,1,128,256]{3,2,1,0:T(8,128)}, f32[48,1,128,256]{3,2,1,0:T(8,128)S(1)}, u32[]{:S(2)}) copy-start(f32[48,1,128,256]{3,2,1,0:T(8,128)S(1)} %multiply_add_fusion) | copy-start | bytes 18874372
  19.6 3.3 %copy-start.8 = (bf16[1,256]{1,0:T(2,128)(2,1)S(1)}, bf16[1,256]{1,0:T(2,128)(2,1)}, u32[]{:S(2)}) copy-start(bf16[1,256]{1,0:T(2,128)(2,1)} %param.30) | copy-start | bytes 1540
  19.6 3.3 %copy-start.2 = (bf16[48,2048]{1,0:T(8,128)(2,1)S(1)}, bf16[48,2048]{1,0:T(8,128)(2,1)}, u32[]{:S(2)}) copy-start(bf16[48,2048]{1,0:T(8,128)(2,1)} %param.21) | copy-start | bytes 589828
  19.6 6.3 %copy-start.5 = (s32[48,2]{0,1:T(2,128)S(1)}, s32[48,2]{0,1:T(2,128)}, u32[]{:S(2)}) copy-start(s32[48,2]{0,1:T(2,128)} %param.34) | copy-start | bytes 1156
  48.6 6.7 %copy-start.3 = (bf16[48,512]{1,0:T(8,128)(2,1)}, bf16[48,512]{1,0:T(8,128)(2,1)S(1)}, u32[]{:S(2)}) copy-start(bf16[48,512]{1,0:T(8,128)(2,1)S(1)} %add_convert_fusion) | copy-start | bytes 147460
  83.0 11.5 %all-to-all-start = ((bf16[8,14,512]{2,1,0:T(8,128)(2,1)}), bf16[8,14,512]{2,1,0:T(8,128)(2,1)}, u32[]{:S(2)}, u32[]{:S(2)}) async-start(bf16[8,14,512]{2,1,0:T(8,128)(2,1)} %reshape.136), calls=%async_computation.2 | async-start | bytes 262144 | tf_op jit(solution)/shard_map/all_to_all | solution.py:108
  88.2 44.7 %all-reduce.3.cloned.1.call-start = ((), (), s32[]{:S(2)}) async-start(), calls=%async_computation.6 | async-start | bytes 1572864 | tf_op jit(solution)/shard_map/psum | solution.py:23
  92.1 65.9 %reduce-scatter.8.cloned.1.call-start = ((), (), s32[]{:S(2)}) async-start(), calls=%async_computation.8 | async-start | bytes 573440 | tf_op jit(solution)/shard_map/reduce_scatter | solution.py:120
  121.3 100.2 %reduce-scatter.6.cloned.1.call-start = ((), (), s32[]{:S(2)}) async-start(), calls=%async_computation.7 | async-start | bytes 442368 | tf_op jit(solution)/shard_map/reduce_scatter | solution.py:139
  134.1 30.7 %copy-start.6 = (pred[48,2]{0,1:T(4,128)(4,1)S(1)}, pred[48,2]{0,1:T(4,128)(4,1)}, u32[]{:S(2)}) copy-start(pred[48,2]{0,1:T(4,128)(4,1)} %get-tuple-element.6) | copy-start | bytes 292
  134.2 31.4 %copy-start.7 = (f32[48,2]{0,1:T(2,128)S(1)}, f32[48,2]{0,1:T(2,128)}, u32[]{:S(2)}) copy-start(f32[48,2]{0,1:T(2,128)} %param.35) | copy-start | bytes 1156
  136.4 85.2 %copy-start.4 = (bf16[48,512]{1,0:T(8,128)(2,1)S(1)}, bf16[48,512]{1,0:T(8,128)(2,1)}, u32[]{:S(2)}) copy-start(bf16[48,512]{1,0:T(8,128)(2,1)} %copy-done.3) | copy-start | bytes 147460
  159.6 11.6 %all-to-all-start.1 = ((bf16[8,14,512]{2,1,0:T(8,128)(2,1)}), bf16[8,14,512]{2,1,0:T(8,128)(2,1)S(1)}, u32[]{:S(2)}, u32[]{:S(2)}) async-start(bf16[8,14,512]{2,1,0:T(8,128)(2,1)} %convert_element_type.131), calls=%async_computation.4 | async-start | bytes 262144 | tf_op jit(solution)/shard_map/all_to_all | solution.py:123
Sparse Core Ops, SparseCore 0:
  26.1 21.5 reduce-scatter.3
  92.2 40.5 all-reduce.2
  135.4 22.5 reduce-scatter.7
  161.1 60.4 reduce-scatter.5
where the time goes:
time: 233 us; the launch traced here: 230 us
  waiting for transfers between devices  105 us (45%)
  blocking collectives  49.3 us (21%)
  matrix products  24.6 us (11%)
  other arithmetic  16.3 us (7%)
  between operations  14 us (6%)
  starting transfers between devices  10.6 us (5%)
  local copies, waits for them, and re-layouts  9.71 us (4%)
    reduce_scatter x1, waiting for transfers between devices, body(): lax.psum_scatter(matmul(dense_hidden, dense_down).astype(jnp.bfloat16), '...  46.8 us
    all_gather x1, blocking collectives, body(): piece = lax.all_gather(ffn_own, 'ep', axis=0, tiled=True)  25.2 us
    dot_general x11, matrix products, matmul(): return jnp.dot(left, right, preferred_element_type=jnp.float32)  21.5 us
    reduce_scatter x1, waiting for transfers between devices, body(): lax.psum_scatter(block_out.astype(jnp.bfloat16), 'tp', scatter_dimension=...  21.4 us
    reduce_scatter x1, waiting for transfers between devices, body(): lax.psum_scatter(partial_out.astype(jnp.bfloat16), 'tp', scatter_dimensio...  18.7 us
    all_gather x1, blocking collectives, body(): lax.all_gather(lax.all_to_all(outgoing, 'ep', split_axis=0, concat_axis=0...  18.2 us
    psum x1, waiting for transfers between devices, unit_totals(): return lax.psum(paired.astype(jnp.bfloat16), 'tp').astype(jnp.float32)  11.5 us
    psum x1, blocking collectives, body(): lax.psum((jnp.sum(middle_own * middle_own, axis=-1), jnp.sum(middle_own *...  6.02 us
  transfers between devices with their start and end apart: 6, of which 6 were waited for; matrix products, arithmetic and copies ran while one was open for 11% of the time, Pallas kernels for 0%

commit v1 on v0

v1 whole, which is shorter than its diff:
```python
import functools

import jax
import jax.numpy as jnp
from jax import lax
from jax.experimental import pallas as pl
from jax.experimental.pallas import tpu as pltpu
from jax.sharding import PartitionSpec as P

EPSILON = 1e-06
TAU_DECAY = 16.0
MESH = pl.DeviceIdType.MESH


def rms_factor(values):
    return lax.rsqrt(jnp.mean(values * values, axis=-1, keepdims=True) + EPSILON)


def matmul(left, right):
    return jnp.dot(left, right, preferred_element_type=jnp.float32)


def silu(values):
    return values * jax.nn.sigmoid(values)


def layer_kernel(
    n_ep,
    n_tp,
    gated_ref,
    outw_ref,
    hid_ref,
    gain_ref,
    gate_ref,
    sel_ref,
    comb_hi_ref,
    comb_lo_ref,
    eg_hbm,
    eu_hbm,
    ed_hbm,
    dg_hbm,
    du_hbm,
    dd_hbm,
    mixed_ref,
    eg,
    eu,
    ed,
    dgw,
    duw,
    ddw,
    sel_recv,
    p_send,
    p_recv,
    st_send,
    st_recv,
    mid_buf,
    br_buf,
    piece,
    rows_all,
    g_send,
    g_recv,
    u_send,
    u_recv,
    e_hid,
    eo_send,
    eo_recv,
    d_hid,
    out_send,
    out_recv,
    ret_send,
    ret,
    w_sem,
    tp_ssem,
    tp_rsem,
    ep_ssem,
    ep_rsem,
):
    f32, bf16 = jnp.float32, jnp.bfloat16
    ep = lax.axis_index("ep")
    tp = lax.axis_index("tp")
    tokens, quarter = hid_ref.shape
    width = quarter * n_tp
    cap = sel_ref.shape[1]

    loads = []
    for i, (src, dst) in enumerate(
        ((dg_hbm, dgw), (du_hbm, duw), (eg_hbm, eg), (eu_hbm, eu), (ed_hbm, ed), (dd_hbm, ddw))
    ):
        load = pltpu.make_async_copy(src, dst, w_sem.at[i])
        load.start()
        loads.append(load)

    barrier = pltpu.get_barrier_semaphore()
    for d in range(1, n_tp):
        pl.semaphore_signal(
            barrier, inc=1, device_id=(ep, lax.rem(tp + d, n_tp)), device_id_type=MESH
        )
    for d in range(1, n_ep):
        pl.semaphore_signal(
            barrier, inc=1, device_id=(lax.rem(ep + d, n_ep), tp), device_id_type=MESH
        )

    def over_tp(phase, src_of, dst_of):
        copies = []
        for d in range(1, n_tp):
            peer = lax.rem(tp + d, n_tp)
            copy = pltpu.make_async_remote_copy(
                src_ref=src_of(peer),
                dst_ref=dst_of(d),
                send_sem=tp_ssem.at[phase, d - 1],
                recv_sem=tp_rsem.at[phase, d - 1],
                device_id=(ep, peer),
                device_id_type=MESH,
            )
            copy.start()
            copies.append(copy)
        return copies

    def over_ep(phase, src_of, dst_of):
        copies = []
        for d in range(1, n_ep):
            peer = lax.rem(ep + d, n_ep)
            copy = pltpu.make_async_remote_copy(
                src_ref=src_of(peer),
                dst_ref=dst_of(d),
                send_sem=ep_ssem.at[phase, d - 1],
                recv_sem=ep_rsem.at[phase, d - 1],
                device_id=(peer, tp),
                device_id_type=MESH,
            )
            copy.start()
            copies.append(copy)
        return copies

    def arrive(copies):
        for copy in copies:
            copy.wait_recv()

    for j in range(n_tp):
        p_send[j] = matmul(gated_ref[...], outw_ref[:, j * quarter : (j + 1) * quarter]).astype(bf16)
    pl.semaphore_wait(barrier, n_tp + n_ep - 2)
    c_part = over_tp(0, lambda peer: p_send.at[peer], lambda d: p_recv.at[d - 1])
    c_sel = over_ep(0, lambda peer: sel_ref.at[peer], lambda d: sel_recv.at[ep])
    sel_recv[ep] = sel_ref[ep]
    attended = p_send[tp].astype(f32)
    for d in range(1, n_tp):
        c_part[d - 1].wait_recv()
        attended = attended + p_recv[d - 1].astype(f32)
    middle = (hid_ref[...].astype(f32) + attended).astype(bf16).astype(f32)
    gain = gain_ref[...]
    squares = jnp.sum(middle * middle, axis=-1, keepdims=True)
    inner = jnp.sum(middle * gain * gate_ref[...], axis=-1, keepdims=True)
    lane = lax.broadcasted_iota(jnp.int32, (tokens, 128), 1)
    st_send[...] = jnp.where(lane < 64, squares, inner)
    c_stat = over_tp(1, lambda peer: st_send, lambda d: st_recv.at[d - 1])
    mid_buf[...] = middle
    totals = st_send[...]
    for d in range(1, n_tp):
        c_stat[d - 1].wait_recv()
        totals = totals + st_recv[d - 1]
    factor = lax.rsqrt(totals[:, 0:1] / width + EPSILON)
    br_buf[...] = jnp.broadcast_to(jax.nn.sigmoid(totals[:, 64:65] * factor), (tokens, 128))
    piece[ep] = (middle * factor * gain).astype(bf16)
    c_piece = over_ep(1, lambda peer: piece.at[ep], lambda d: piece.at[ep])

    arrive(c_sel)
    for d in range(n_ep):
        if d:
            c_piece[d - 1].wait_recv()
        source = lax.rem(ep - d + n_ep, n_ep)
        picked = matmul(sel_recv[source][:, :tokens], piece[source]).astype(bf16)
        rows_all[tp, pl.ds(pl.multiple_of(source * cap, cap), cap), :] = picked
    c_rows = over_tp(2, lambda peer: rows_all.at[tp], lambda d: rows_all.at[tp])

    loads[0].wait()
    loads[1].wait()
    everyone = piece[...].reshape(n_ep * tokens, quarter)
    units = dgw.shape[1]
    share = n_ep * tokens // n_tp
    g_send[...] = matmul(everyone, dgw[...]).astype(bf16).reshape(n_tp, share, units)
    c_g = over_tp(3, lambda peer: g_send.at[peer], lambda d: g_recv.at[d - 1])
    u_send[...] = matmul(everyone, duw[...]).astype(bf16).reshape(n_tp, share, units)
    c_u = over_tp(4, lambda peer: u_send.at[peer], lambda d: u_recv.at[d - 1])

    loads[2].wait()
    loads[3].wait()
    arrive(c_rows)
    block = eg.shape[1]
    tile = 256 if block % 256 == 0 else 128

    @pl.loop(0, block // tile)
    def _(i):
        cols = pl.ds(pl.multiple_of(i * tile, tile), tile)
        gate_part = matmul(rows_all[0], eg[0:quarter, cols])
        up_part = matmul(rows_all[0], eu[0:quarter, cols])
        for j in range(1, n_tp):
            span = slice(j * quarter, (j + 1) * quarter)
            gate_part = gate_part + matmul(rows_all[j], eg[span, cols])
            up_part = up_part + matmul(rows_all[j], eu[span, cols])
        e_hid[:, cols] = (silu(gate_part) * up_part).astype(bf16)

    g_sum = g_send[tp].astype(f32)
    u_sum = u_send[tp].astype(f32)
    for d in range(1, n_tp):
        c_g[d - 1].wait_recv()
        g_sum = g_sum + g_recv[d - 1].astype(f32)
    for d in range(1, n_tp):
        c_u[d - 1].wait_recv()
        u_sum = u_sum + u_recv[d - 1].astype(f32)
    d_hid[tp] = (silu(g_sum) * u_sum).astype(bf16)
    c_hid = over_tp(5, lambda peer: d_hid.at[tp], lambda d: d_hid.at[tp])

    loads[4].wait()
    for j in range(n_tp):
        eo_send[j] = matmul(e_hid[...], ed[:, j * quarter : (j + 1) * quarter]).astype(bf16)
    c_eo = over_tp(6, lambda peer: eo_send.at[peer], lambda d: eo_recv.at[d - 1])

    loads[5].wait()
    arrive(c_hid)
    hidden = d_hid[...].reshape(n_ep * tokens, units)
    out_send[...] = matmul(hidden, ddw[...]).astype(bf16).reshape(n_ep, tokens, quarter)
    c_out = over_ep(2, lambda peer: out_send.at[peer], lambda d: out_recv.at[d - 1])

    summed = eo_send[tp].astype(f32)
    for d in range(1, n_tp):
        c_eo[d - 1].wait_recv()
        summed = summed + eo_recv[d - 1].astype(f32)
    ret_send[...] = summed.astype(bf16).reshape(n_ep, cap, quarter)
    c_ret = over_ep(3, lambda peer: ret_send.at[peer], lambda d: ret.at[ep])
    ret[ep] = ret_send[ep]

    dense = out_send[ep].astype(f32)
    for d in range(1, n_ep):
        c_out[d - 1].wait_recv()
        dense = dense + out_recv[d - 1].astype(f32)
    arrive(c_ret)
    answers = ret[...].reshape(n_ep * cap, quarter)
    routed = matmul(comb_hi_ref[...], answers) + matmul(comb_lo_ref[...], answers)
    mixed_ref[...] = (mid_buf[...] + br_buf[:, 0:1] * dense + routed).astype(bf16)

    for copies in (c_part, c_sel, c_stat, c_piece, c_rows, c_g, c_u, c_hid, c_eo, c_out, c_ret):
        for copy in copies:
            copy.wait_send()


def run_layer(gated, output_weight, hid, gain, gate, sel, comb_hi, comb_lo, eg, eu, ed, dg, du, dd):
    n_ep, n_tp = lax.axis_size("ep"), lax.axis_size("tp")
    tokens, quarter = hid.shape
    cap = sel.shape[1]
    items = n_ep * cap
    share = n_ep * tokens // n_tp
    units = dg.shape[1]
    bf16, f32 = jnp.bfloat16, jnp.float32
    vmem = pl.BlockSpec(memory_space=pltpu.VMEM)
    anyspace = pl.BlockSpec(memory_space=pl.ANY)
    scratch = [pltpu.VMEM(w.shape, bf16) for w in (eg, eu, ed, dg, du, dd)]
    scratch += [
        pltpu.VMEM(sel.shape, bf16),
        pltpu.VMEM((n_tp, tokens, quarter), bf16),
        pltpu.VMEM((n_tp - 1, tokens, quarter), bf16),
        pltpu.VMEM((tokens, 128), f32),
        pltpu.VMEM((n_tp - 1, tokens, 128), f32),
        pltpu.VMEM((tokens, quarter), f32),
        pltpu.VMEM((tokens, 128), f32),
        pltpu.VMEM((n_ep, tokens, quarter), bf16),
        pltpu.VMEM((n_tp, items, quarter), bf16),
        pltpu.VMEM((n_tp, share, units), bf16),
        pltpu.VMEM((n_tp - 1, share, units), bf16),
        pltpu.VMEM((n_tp, share, units), bf16),
        pltpu.VMEM((n_tp - 1, share, units), bf16),
        pltpu.VMEM((items, eg.shape[1]), bf16),
        pltpu.VMEM((n_tp, items, quarter), bf16),
        pltpu.VMEM((n_tp - 1, items, quarter), bf16),
        pltpu.VMEM((n_tp, share, units), bf16),
        pltpu.VMEM((n_ep, tokens, quarter), bf16),
        pltpu.VMEM((n_ep - 1, tokens, quarter), bf16),
        pltpu.VMEM((n_ep, cap, quarter), bf16),
        pltpu.VMEM((n_ep, cap, quarter), bf16),
        pltpu.SemaphoreType.DMA((6,)),
        pltpu.SemaphoreType.DMA((7, n_tp - 1)),
        pltpu.SemaphoreType.DMA((7, n_tp - 1)),
        pltpu.SemaphoreType.DMA((4, n_ep - 1)),
        pltpu.SemaphoreType.DMA((4, n_ep - 1)),
    ]
    return pl.pallas_call(
        functools.partial(layer_kernel, n_ep, n_tp),
        out_shape=jax.ShapeDtypeStruct((tokens, quarter), bf16),
        in_specs=[vmem] * 8 + [anyspace] * 6,
        out_specs=vmem,
        scratch_shapes=scratch,
        compiler_params=pltpu.CompilerParams(
            collective_id=0, has_side_effects=True, vmem_limit_bytes=60 * 1024 * 1024
        ),
    )(gated, output_weight, hid, gain, gate, sel, comb_hi, comb_lo, eg, eu, ed, dg, du, dd)


def body(
    hidden_in,
    carried_state,
    input_gain,
    query_weight,
    key_weight,
    value_weight,
    outgate_weight,
    decay_weight,
    decay_shift,
    head_gain,
    output_weight,
    channel_gain,
    branch_gate,
    routes,
    route_weights,
    expert_gate,
    expert_up,
    expert_down,
    dense_gate,
    dense_up,
    dense_down,
):
    tokens_here, width = hidden_in.shape
    heads_here, key_dim, value_dim = carried_state.shape[1:]
    quarter = width // lax.axis_size("tp")
    lane_start = lax.axis_index("tp") * quarter
    inputs = hidden_in.astype(jnp.float32)
    normed = (inputs * rms_factor(inputs) * input_gain.astype(jnp.float32)).astype(jnp.bfloat16)
    query = matmul(normed, query_weight).astype(jnp.bfloat16)
    key_rows = matmul(normed, key_weight).astype(jnp.bfloat16)
    value_rows = matmul(normed, value_weight).astype(jnp.bfloat16)
    outgate = matmul(normed, outgate_weight).astype(jnp.bfloat16)
    decay = jnp.exp(jax.nn.log_sigmoid(matmul(normed, decay_weight)) / TAU_DECAY + decay_shift)
    decay = decay.reshape(tokens_here, heads_here, key_dim)
    query_scaled = query.astype(jnp.float32).reshape(
        tokens_here, heads_here, key_dim
    ) * key_dim ** (-0.5)
    key_vals = key_rows.astype(jnp.float32).reshape(tokens_here, heads_here, key_dim)
    value_vals = value_rows.astype(jnp.float32).reshape(tokens_here, heads_here, value_dim)
    new_state = decay[..., None] * carried_state + key_vals[..., None] * value_vals[:, :, None, :]
    readout = jnp.einsum("bhk,bhkv->bhv", query_scaled, new_state, precision=lax.Precision.HIGHEST)
    gate_vals = jax.nn.silu(outgate.astype(jnp.float32).reshape(tokens_here, heads_here, value_dim))
    gated = (readout * rms_factor(readout) * head_gain.astype(jnp.float32) * gate_vals).astype(
        jnp.bfloat16
    )
    gated = gated.reshape(tokens_here, heads_here * value_dim)
    hid_own = lax.dynamic_slice_in_dim(hidden_in, lane_start, quarter, 1)
    own_gain = lax.dynamic_slice_in_dim(channel_gain, lane_start, quarter, 0)
    own_branch = lax.dynamic_slice_in_dim(branch_gate, lane_start, quarter, 0)
    expert_count = lax.axis_size("ep")
    topk = routes.shape[1]
    capacity = tokens_here * topk // expert_count + 2
    cap = (capacity + 15) // 16 * 16
    chosen = (
        routes[:, :, None] == jnp.arange(expert_count, dtype=jnp.int32)[None, None, :]
    ).astype(jnp.int32)
    chosen_flat = chosen.reshape(tokens_here * topk, expert_count)
    index = jnp.arange(tokens_here * topk, dtype=jnp.int32)
    before = (index[:, None] > index[None, :]).astype(jnp.bfloat16)
    earlier = matmul(before, chosen_flat.astype(jnp.bfloat16))
    slot_index = jnp.sum(earlier * chosen_flat, axis=1).astype(jnp.int32)
    position = routes * cap + slot_index.reshape(tokens_here, topk)
    slot_table = jnp.arange(expert_count * cap, dtype=jnp.int32)
    sel = jnp.sum((slot_table[:, None, None] == position[None, :, :]).astype(jnp.float32), axis=2)
    sel = jnp.pad(sel, ((0, 0), (0, -tokens_here % 128))).astype(jnp.bfloat16)
    sel = sel.reshape(expert_count, cap, sel.shape[1])
    comb = jnp.sum(
        jnp.where(position[:, :, None] == slot_table, route_weights[:, :, None], 0.0), axis=1
    )
    comb_hi = lax.optimization_barrier(comb.astype(jnp.bfloat16))
    comb_lo = (comb - comb_hi.astype(jnp.float32)).astype(jnp.bfloat16)
    mixed = run_layer(
        gated,
        output_weight,
        hid_own,
        own_gain.astype(jnp.float32)[None, :],
        own_branch.astype(jnp.float32)[None, :],
        sel,
        comb_hi,
        comb_lo,
        expert_gate[0],
        expert_up[0],
        expert_down[0],
        dense_gate,
        dense_up,
        dense_down,
    )
    return (mixed, new_state)


def solution(mesh):
    in_specs = (
        P("ep", None),
        P("ep", "tp", None, None),
        P(),
        P(None, "tp"),
        P(None, "tp"),
        P(None, "tp"),
        P(None, "tp"),
        P(None, "tp"),
        P("ep", "tp"),
        P("tp", None),
        P("tp", None),
        P(),
        P(),
        P("ep", None),
        P("ep", None),
        P("ep", None, "tp"),
        P("ep", None, "tp"),
        P("ep", "tp", None),
        P("tp", "ep"),
        P("tp", "ep"),
        P("ep", "tp"),
    )
    out_specs = (P("ep", "tp"), P("ep", "tp", None, None))
    return jax.shard_map(body, mesh=mesh, in_specs=in_specs, out_specs=out_specs, check_vma=False)
```

time: 233 us -> 81.4 us (0.35); the launches traced: 230 us -> 81.1 us
  waiting for transfers between devices: 105 us -> 0 us
  Pallas kernels: 0 us -> 57.4 us
  blocking collectives: 49.3 us -> 0 us
  matrix products: 24.6 us -> 8.54 us
  between operations: 14 us -> 0.85 us
  starting transfers between devices: 10.6 us -> 0 us
  other arithmetic: 16.3 us -> 8.66 us
  local copies, waits for them, and re-layouts: 9.71 us -> 5.63 us
    reduce_scatter x3 -> x0, waiting for transfers between devices: 86.8 us -> none  [the longest x1 46.8 us: body(): lax.psum_scatter(matmul(dense_hidden, dense_down).astype(jnp.bfloat16), '...]
    pallas_call x0 -> x1, Pallas kernels: none -> 57.4 us  [run_layer(): pl.pallas_call(functools.partial(layer_kernel, n_ep, n_tp), out_shape=jax...]
    all_gather x2 -> x0, blocking collectives: 43.3 us -> none  [the longest x1 25.2 us: body(): piece = lax.all_gather(ffn_own, 'ep', axis=0, tiled=True)]
    dot_general x11 -> x6, matrix products: 21.5 us -> 5.45 us  [matmul(): return jnp.dot(left, right, preferred_element_type=jnp.float32)]
    psum x1 -> x0, waiting for transfers between devices: 11.5 us -> none  [unit_totals(): return lax.psum(paired.astype(jnp.bfloat16), 'tp').astype(jnp.float32)]
    all_to_all x2 -> x0, starting transfers between devices: 10.4 us -> none  [the longest x1 5.24 us: body(): lax.all_to_all(summed.reshape(sources, items, quarter).astype(jnp.bfloat1...]
    all_to_all x2 -> x0, waiting for transfers between devices: 6.68 us -> none  [the longest x1 4.34 us: body(): lax.all_to_all(summed.reshape(sources, items, quarter).astype(jnp.bfloat1...]
    psum x1 -> x0, blocking collectives: 6.02 us -> none  [body(): lax.psum((jnp.sum(middle_own * middle_own, axis=-1), jnp.sum(middle_own *...]
  transfers between devices with their start and end apart: 6 -> 0, of which waited for: 6 -> 0; matrix products, arithmetic and copies ran while one was open for 11% -> 0% of each run, Pallas kernels for 0% -> 0%
where the time goes in v1:
time: 81.4 us; the launch traced here: 81.1 us
  Pallas kernels  57.4 us (71%)
  other arithmetic  8.66 us (11%)
  matrix products  8.54 us (10%)
  local copies, waits for them, and re-layouts  5.63 us (7%)
  between operations  0.85 us (1%)
    pallas_call x1, Pallas kernels, run_layer(): pl.pallas_call(functools.partial(layer_kernel, n_ep, n_tp), out_shape=jax...  57.4 us
    dot_general x6, matrix products, matmul(): return jnp.dot(left, right, preferred_element_type=jnp.float32)  5.45 us
    add x1, other arithmetic, body(): decay[..., None] * carried_state  4.52 us
    unnamed x21, local copies, waits for them, and re-layouts  4.05 us
    dot_general x1, matrix products, body(): jnp.einsum('bhk,bhkv->bhv', query_scaled, new_state, precision=lax.Precis...  3.09 us

profile of v1, /device:TPU:1, one launch (start us, length us, event | category | flops | bytes accessed | tf_op | source)
XLA Modules:
  0.0 81.1 jit_solution(11560196318443108084)
XLA Ops:
  0.6 0.0 copy-start
  0.6 0.8 convert_element_type.74
  1.4 1.1 %fusion.8 = f32[48]{0:T(128)S(1)} fusion(bf16[48,2048]{1,0:T(8,128)(2,1)} %param.21), kind=kLoop, calls=%fused_computation.17 | loop fusion | flops 294864 | bytes 196800 | tf_op jit(solution)/shard_map/reduce_sum | solution.py:16
  2.5 0.0 copy-done
  2.5 1.3 %fusion.3 = f32[48,256]{1,0:T(8,128)S(1)} fusion(bf16[2048,256]{1,0:T(8,128)(2,1)S(1)} %copy-done, bf16[48,2048]{1,0:T(8,128)(2,1)} %param.21, f32[2048]{0:T(1024)S(1)} %convert_element_type.74, f32[48]{0:T(128)S(1)} %add_rsqrt_fusion.1), kind=kOutput, calls=%fused_computation.6 | convolution fusion | flops 50749440 | bytes 1302720 | tf_op jit(solution)/shard_map/dot_general | solution.py:20
  3.8 1.4 %fusion.18 = f32[48,128]{1,0:T(8,128)S(1)} fusion(f32[48,128]{1,0:T(8,128)} %param.29, bf16[2048,128]{1,0:T(8,128)(2,1)} %param.28, bf16[48,2048]{1,0:T(8,128)(2,1)} %param.21, f32[2048]{0:T(1024)S(1)} %convert_element_type.74, f32[48]{0:T(128)S(1)} %add_rsqrt_fusion.1), kind=kOutput, calls=%fused_computation.35 | convolution fusion | flops 25620480 | bytes 778432 | tf_op jit(solution)/shard_map/dot_general | solution.py:20
  5.2 1.4 %fusion.4 = f32[48,128]{1,0:T(8,128)S(1)} fusion(bf16[2048,128]{1,0:T(8,128)(2,1)} %param.25, bf16[48,2048]{1,0:T(8,128)(2,1)} %param.21, f32[2048]{0:T(1024)S(1)} %convert_element_type.74, f32[48]{0:T(128)S(1)} %add_rsqrt_fusion.1), kind=kOutput, calls=%fused_computation.9 | convolution fusion | flops 25571328 | bytes 753856 | tf_op jit(solution)/shard_map/dot_general | solution.py:20
  6.6 0.0 copy-start.2
  6.6 0.0 copy-start.4
  6.6 4.5 %multiply_add_fusion = f32[48,1,128,256]{3,2,1,0:T(8,128)S(1)} fusion(f32[48,1,128,256]{3,2,1,0:T(8,128)} %param.22, f32[48,256]{1,0:T(8,128)S(1)} %fusion.3, f32[48,128]{1,0:T(8,128)S(1)} %fusion.4, f32[48,128]{1,0:T(8,128)S(1)} %fusion.18), kind=kLoop, calls=%fused_computation.2 | loop fusion | flops 4718592 | bytes 12681216 | tf_op jit(solution)/shard_map/add | solution.py:337
  11.2 0.0 copy-done.2
  11.2 0.0 copy-done.4
  11.2 0.0 copy-start.1
  11.2 0.0 copy-start.7
  11.2 0.0 copy-start.3
  11.2 0.0 copy-start.6
  11.2 0.0 copy-start.8
  11.2 0.3 fusion.6
  11.5 2.4 %copy-done.1 = f32[48,1,128,256]{3,2,1,0:T(8,128)} copy-done((f32[48,1,128,256]{3,2,1,0:T(8,128)}, f32[48,1,128,256]{3,2,1,0:T(8,128)S(1)}, u32[]{:S(2)}) %copy-start.1) | copy-done | bytes 6291480
  13.9 3.1 %fusion = f32[48,1,256]{2,1,0:T(1,128)S(1)} fusion(f32[48,128,1]{1,2,0:T(1,128)S(1)} %bitcast.34, f32[48,1,128,256]{3,2,1,0:T(8,128)S(1)} %multiply_add_fusion), kind=kOutput, calls=%fused_computation | convolution fusion | flops 18874368 | bytes 6365184 | tf_op jit(solution)/shard_map/bhk,bhkv->bhv/dot_general | solution.py:338
  17.0 0.1 fusion.11
  17.1 0.0 copy-done.7
  17.1 0.0 copy-done.3
  17.1 1.0 %fusion.14.gated_ref = bf16[48,256]{1,0:T(8,128)(2,1)} fusion(bf16[2048,256]{1,0:T(8,128)(2,1)S(1)} %copy-done.3, f32[48,1,256]{2,1,0:T(1,128)S(1)} %fusion, f32[256]{0:T(256)S(1)} %bitcast.37, f32[48]{0:T(128)S(1)} %add_rsqrt_fusion, bf16[48,2048]{1,0:T(8,128)(2,1)S(1)} %copy-done.2, f32[2048]{0:T(1024)S(1)} %convert_element_type.74, ...), kind=kOutput, calls=%fused_computation.26 | convolution fusion | flops 50847744 | bytes 1328512 | tf_op jit(solution)/shard_map/dot_general | solution.py:20
  18.1 1.4 %dynamic-slice_convert_fusion = (f32[512]{0:T(512)}, f32[512]{0:T(512)}) fusion(bf16[2048]{0:T(1024)(128)(2,1)} %param.33, s32[]{:T(128)S(6)} %select_n.15, bf16[2048]{0:T(1024)(128)(2,1)} %param.32), kind=kLoop, calls=%fused_computation.42 | loop fusion | flops 1024 | bytes 6148 | tf_op jit(solution)/shard_map/broadcast_in_dim | solution.py:374
  19.5 0.6 constant_dynamic-slice_fusion.hid_ref
  20.1 0.0 copy-done.6
  20.1 0.1 copy.37
  20.2 0.1 eq.43
  20.3 0.1 fusion.7
  20.5 0.1 convert_element_type.89
  20.6 0.1 copy.38
  20.7 0.0 copy-done.8
  20.7 0.1 select_reduce_fusion
  20.8 0.0 copy-start.5
  20.8 0.6 subtract_convert_fusion.comb_lo_ref
  21.4 0.1 convert_reduce_fusion
  21.5 0.1 copy.42
  21.6 0.6 pad.5.clone
  22.2 0.0 copy-done.5
  22.3 57.4 %shard_map.212 = bf16[48,512]{1,0:T(8,128)(2,1)} custom-call(bf16[48,256]{1,0:T(8,128)(2,1)} %fusion.14.gated_ref, bf16[256,2048]{1,0:T(8,128)(2,1)} %outw_ref.1, bf16[48,512]{1,0:T(8,128)(2,1)} %constant_dynamic-slice_fusion.hid_ref, f32[1,512]{1,0:T(1,128)} %bitcast.36, f32[1,512]{1,0:T(1,128)} %bitcast.35, bf16[8,16,128]{2,1,0:T(8,128)(2,1)} %bitcast.33, ...), custom_call_target="tpu_custom_call" | custom-call | tf_op jit(solution)/shard_map/pallas_call | solution.py:285
  79.6 1.4 %copy.46 = bf16[48,512]{1,0:T(8,128)(2,1)} copy(bf16[48,512]{1,0:T(8,128)(2,1)} %shard_map.212) | data formatting | bytes 98304
  (6 shorter events, 0.0 us)
Async XLA Ops:
  0.6 1.9 %copy-start = (bf16[2048,256]{1,0:T(8,128)(2,1)S(1)}, bf16[2048,256]{1,0:T(8,128)(2,1)}, u32[]{:S(2)}) copy-start(bf16[2048,256]{1,0:T(8,128)(2,1)} %param.26) | copy-start | bytes 3145732
  6.6 4.6 %copy-start.2 = (bf16[48,2048]{1,0:T(8,128)(2,1)S(1)}, bf16[48,2048]{1,0:T(8,128)(2,1)}, u32[]{:S(2)}) copy-start(bf16[48,2048]{1,0:T(8,128)(2,1)} %param.21) | copy-start | bytes 589828
  6.6 4.5 %copy-start.4 = (bf16[2048,128]{1,0:T(8,128)(2,1)S(1)}, bf16[2048,128]{1,0:T(8,128)(2,1)}, u32[]{:S(2)}) copy-start(bf16[2048,128]{1,0:T(8,128)(2,1)} %param.24) | copy-start | bytes 1572868
  11.2 2.7 %copy-start.1 = (f32[48,1,128,256]{3,2,1,0:T(8,128)}, f32[48,1,128,256]{3,2,1,0:T(8,128)S(1)}, u32[]{:S(2)}) copy-start(f32[48,1,128,256]{3,2,1,0:T(8,128)S(1)} %multiply_add_fusion) | copy-start | bytes 18874372
  11.2 5.9 %copy-start.7 = (bf16[1,256]{1,0:T(2,128)(2,1)S(1)}, bf16[1,256]{1,0:T(2,128)(2,1)}, u32[]{:S(2)}) copy-start(bf16[1,256]{1,0:T(2,128)(2,1)} %param.30) | copy-start | bytes 1540
  11.2 5.9 %copy-start.3 = (bf16[2048,256]{1,0:T(8,128)(2,1)S(1)}, bf16[2048,256]{1,0:T(8,128)(2,1)}, u32[]{:S(2)}) copy-start(bf16[2048,256]{1,0:T(8,128)(2,1)} %param.27) | copy-start | bytes 3145732
  11.2 8.9 %copy-start.6 = (s32[48,2]{0,1:T(2,128)S(1)}, s32[48,2]{0,1:T(2,128)}, u32[]{:S(2)}) copy-start(s32[48,2]{0,1:T(2,128)} %param.34) | copy-start | bytes 1156
  11.2 9.5 %copy-start.8 = (f32[48,2]{0,1:T(2,128)S(1)}, f32[48,2]{0,1:T(2,128)}, u32[]{:S(2)}) copy-start(f32[48,2]{0,1:T(2,128)} %param.35) | copy-start | bytes 1156
  20.8 1.4 %copy-start.5 = (bf16[48,128]{1,0:T(8,128)(2,1)}, bf16[48,128]{1,0:T(8,128)(2,1)S(1)}, u32[]{:S(2)}) copy-start(bf16[48,128]{1,0:T(8,128)(2,1)S(1)} %convert_element_type.91.comb_hi_ref) | copy-start | bytes 36868

commit v2 on v1

--- a/solution.py
+++ b/solution.py
@@ -78,8 +78,9 @@
     f32, bf16 = jnp.float32, jnp.bfloat16
     ep = lax.axis_index("ep")
     tp = lax.axis_index("tp")
-    tokens, quarter = hid_ref.shape
-    width = quarter * n_tp
+    tokens, width = hid_ref.shape
+    quarter = width // n_tp
+    own = pl.ds(pl.multiple_of(tp * quarter, quarter), quarter)
     cap = sel_ref.shape[1]
 
     loads = []
@@ -146,10 +147,10 @@
     for d in range(1, n_tp):
         c_part[d - 1].wait_recv()
         attended = attended + p_recv[d - 1].astype(f32)
-    middle = (hid_ref[...].astype(f32) + attended).astype(bf16).astype(f32)
-    gain = gain_ref[...]
+    middle = (hid_ref[:, own].astype(f32) + attended).astype(bf16).astype(f32)
+    gain = gain_ref[:, own].astype(f32)
     squares = jnp.sum(middle * middle, axis=-1, keepdims=True)
-    inner = jnp.sum(middle * gain * gate_ref[...], axis=-1, keepdims=True)
+    inner = jnp.sum(middle * gain * gate_ref[:, own].astype(f32), axis=-1, keepdims=True)
     lane = lax.broadcasted_iota(jnp.int32, (tokens, 128), 1)
     st_send[...] = jnp.where(lane < 64, squares, inner)
     c_stat = over_tp(1, lambda peer: st_send, lambda d: st_recv.at[d - 1])
@@ -245,7 +246,8 @@
 
 def run_layer(gated, output_weight, hid, gain, gate, sel, comb_hi, comb_lo, eg, eu, ed, dg, du, dd):
     n_ep, n_tp = lax.axis_size("ep"), lax.axis_size("tp")
-    tokens, quarter = hid.shape
+    tokens = hid.shape[0]
+    quarter = hid.shape[1] // n_tp
     cap = sel.shape[1]
     items = n_ep * cap
     share = n_ep * tokens // n_tp
@@ -294,6 +296,176 @@
     )(gated, output_weight, hid, gain, gate, sel, comb_hi, comb_lo, eg, eu, ed, dg, du, dd)
 
 
+def attention_kernel(
+    cap,
+    hidden_ref,
+    gain_ref,
+    shift_ref,
+    head_gain_ref,
+    routes_ref,
+    weights_ref,
+    qw_hbm,
+    kw_hbm,
+    vw_hbm,
+    ow_hbm,
+    fw_hbm,
+    state_hbm,
+    gated_ref,
+    sel_ref,
+    comb_hi_ref,
+    comb_lo_ref,
+    new_hbm,
+    qw,
+    kw,
+    vw,
+    ow,
+    fw,
+    state,
+    query,
+    key,
+    value,
+    decay,
+    readout,
+    w_sem,
+    in_sem,
+    out_sem,
+):
+    f32, bf16 = jnp.float32, jnp.bfloat16
+    tokens = hidden_ref.shape[0]
+    heads, key_dim, value_dim = state.shape[1:]
+    groups = tokens // 8
+    loads = []
+    pairs = ((fw_hbm, fw), (kw_hbm, kw), (qw_hbm, qw), (vw_hbm, vw), (ow_hbm, ow))
+    for i, (src, dst) in enumerate(pairs):
+        load = pltpu.make_async_copy(src, dst, w_sem.at[i])
+        load.start()
+        loads.append(load)
+
+    def fetch(g):
+        rows = pl.ds(g * 8, 8)
+        return pltpu.make_async_copy(state_hbm.at[rows], state.at[rows], in_sem.at[g])
+
+    def put(g):
+        rows = pl.ds(g * 8, 8)
+        return pltpu.make_async_copy(state.at[rows], new_hbm.at[rows], out_sem.at[g])
+
+    for g in range(groups):
+        fetch(g).start()
+
+    inputs = hidden_ref[...].astype(f32)
+    normed = (inputs * rms_factor(inputs) * gain_ref[...].astype(f32)).astype(bf16)
+
+    items = comb_hi_ref.shape[1]
+    lane = lax.broadcasted_iota(jnp.int32, (tokens, 128), 1)
+    first, second = routes_ref[:, 0:1], routes_ref[:, 1:2]
+    chosen0 = jnp.where(lane == first, 1.0, 0.0)
+    chosen1 = jnp.where(lane == second, 1.0, 0.0)
+    row = lax.broadcasted_iota(jnp.int32, (tokens, tokens), 0)
+    col = lax.broadcasted_iota(jnp.int32, (tokens, tokens), 1)
+    before = jnp.where(row > col, 1.0, 0.0).astype(bf16)
+    earlier = matmul(before, (chosen0 + chosen1).astype(bf16))
+    slot0 = jnp.sum(earlier * chosen0, axis=1, keepdims=True)
+    slot1 = jnp.sum(earlier * chosen1, axis=1, keepdims=True)
+    table = lax.broadcasted_iota(jnp.int32, (tokens, items), 1)
+    hit0 = table == first * cap + slot0.astype(jnp.int32)
+    hit1 = table == second * cap + slot1.astype(jnp.int32)
+    comb = jnp.where(hit0, weights_ref[:, 0:1], 0.0) + jnp.where(hit1, weights_ref[:, 1:2], 0.0)
+    comb_hi = comb.astype(bf16)
+    comb_hi_ref[...] = comb_hi
+    comb_lo_ref[...] = (comb - comb_hi.astype(f32)).astype(bf16)
+    onehot = (jnp.where(hit0, 1.0, 0.0) + jnp.where(hit1, 1.0, 0.0)).astype(bf16)
+    lanes = sel_ref.shape[1]
+    eye_row = lax.broadcasted_iota(jnp.int32, (tokens, lanes), 0)
+    eye_col = lax.broadcasted_iota(jnp.int32, (tokens, lanes), 1)
+    eye = jnp.where(eye_row == eye_col, 1.0, 0.0).astype(bf16)
+    sel_ref[...] = lax.dot_general(
+        onehot, eye, (((0,), (0,)), ((), ())), preferred_element_type=f32
+    ).astype(bf16)
+
+    def rounded_rows(weight):
+        return matmul(normed, weight[...]).astype(bf16).astype(f32)
+
+    loads[0].wait()
+    drive = matmul(normed, fw[...])
+    log_sig = jnp.minimum(drive, 0.0) - jnp.log1p(jnp.exp(-jnp.abs(drive)))
+    decay[...] = jnp.exp(log_sig / TAU_DECAY + shift_ref[...]).reshape(decay.shape)
+    loads[1].wait()
+    key[...] = rounded_rows(kw).reshape(key.shape)
+    loads[2].wait()
+    query[...] = (rounded_rows(qw) * key_dim ** (-0.5)).reshape(query.shape)
+    loads[3].wait()
+    value[...] = rounded_rows(vw).reshape(value.shape)
+
+    @pl.loop(0, groups)
+    def _(g):
+        fetch(g).wait()
+        for h in range(heads):
+            keys = slice(h * key_dim, (h + 1) * key_dim)
+            vals = slice(h * value_dim, (h + 1) * value_dim)
+            decay_cols = jnp.transpose(decay[g, :, keys])
+            key_cols = jnp.transpose(key[g, :, keys])
+            query_cols = jnp.transpose(query[g, :, keys])
+            for j in range(8):
+                fresh = (
+                    decay_cols[:, j : j + 1] * state[g * 8 + j, h]
+                    + key_cols[:, j : j + 1] * value[g, j : j + 1, vals]
+                )
+                state[g * 8 + j, h] = fresh
+                readout[g, j : j + 1, vals] = jnp.sum(
+                    query_cols[:, j : j + 1] * fresh, axis=0, keepdims=True
+                )
+        put(g).start()
+
+    loads[4].wait()
+    outgate = rounded_rows(ow)
+    out = readout[...].reshape(tokens, heads * value_dim)
+    for h in range(heads):
+        vals = slice(h * value_dim, (h + 1) * value_dim)
+        part = out[:, vals]
+        gain = head_gain_ref[:, vals].astype(f32)
+        gated_ref[:, vals] = (part * rms_factor(part) * gain * silu(outgate[:, vals])).astype(bf16)
+    for g in range(groups):
+        put(g).wait()
+
+
+def run_attention(hidden, gain, shift, head_gain, routes, weights, qw, kw, vw, ow, fw, state, n_ep):
+    bf16, f32 = jnp.bfloat16, jnp.float32
+    tokens, heads, key_dim, value_dim = state.shape
+    capacity = tokens * routes.shape[1] // n_ep + 2
+    cap = (capacity + 15) // 16 * 16
+    items = n_ep * cap
+    groups = tokens // 8
+    lanes = (tokens + 127) // 128 * 128
+    vmem = pl.BlockSpec(memory_space=pltpu.VMEM)
+    anyspace = pl.BlockSpec(memory_space=pl.ANY)
+    gated, sel, comb_hi, comb_lo, new_state = pl.pallas_call(
+        functools.partial(attention_kernel, cap),
+        out_shape=(
+            jax.ShapeDtypeStruct((tokens, heads * value_dim), bf16),
+            jax.ShapeDtypeStruct((items, lanes), bf16),
+            jax.ShapeDtypeStruct((tokens, items), bf16),
+            jax.ShapeDtypeStruct((tokens, items), bf16),
+            jax.ShapeDtypeStruct(state.shape, f32),
+        ),
+        in_specs=[vmem] * 6 + [anyspace] * 6,
+        out_specs=(vmem, vmem, vmem, vmem, anyspace),
+        scratch_shapes=[pltpu.VMEM(w.shape, bf16) for w in (qw, kw, vw, ow, fw)]
+        + [
+            pltpu.VMEM(state.shape, f32),
+            pltpu.VMEM((groups, 8, heads * key_dim), f32),
+            pltpu.VMEM((groups, 8, heads * key_dim), f32),
+            pltpu.VMEM((groups, 8, heads * value_dim), f32),
+            pltpu.VMEM((groups, 8, heads * key_dim), f32),
+            pltpu.VMEM((groups, 8, heads * value_dim), f32),
+            pltpu.SemaphoreType.DMA((5,)),
+            pltpu.SemaphoreType.DMA((groups,)),
+            pltpu.SemaphoreType.DMA((groups,)),
+        ],
+        compiler_params=pltpu.CompilerParams(vmem_limit_bytes=60 * 1024 * 1024),
+    )(hidden, gain, shift, head_gain, routes, weights, qw, kw, vw, ow, fw, state)
+    return gated, sel.reshape(n_ep, cap, lanes), comb_hi, comb_lo, new_state
+
+
 def body(
     hidden_in,
     carried_state,
@@ -317,61 +489,27 @@
     dense_up,
     dense_down,
 ):
-    tokens_here, width = hidden_in.shape
-    heads_here, key_dim, value_dim = carried_state.shape[1:]
-    quarter = width // lax.axis_size("tp")
-    lane_start = lax.axis_index("tp") * quarter
-    inputs = hidden_in.astype(jnp.float32)
-    normed = (inputs * rms_factor(inputs) * input_gain.astype(jnp.float32)).astype(jnp.bfloat16)
-    query = matmul(normed, query_weight).astype(jnp.bfloat16)
-    key_rows = matmul(normed, key_weight).astype(jnp.bfloat16)
-    value_rows = matmul(normed, value_weight).astype(jnp.bfloat16)
-    outgate = matmul(normed, outgate_weight).astype(jnp.bfloat16)
-    decay = jnp.exp(jax.nn.log_sigmoid(matmul(normed, decay_weight)) / TAU_DECAY + decay_shift)
-    decay = decay.reshape(tokens_here, heads_here, key_dim)
-    query_scaled = query.astype(jnp.float32).reshape(
-        tokens_here, heads_here, key_dim
-    ) * key_dim ** (-0.5)
-    key_vals = key_rows.astype(jnp.float32).reshape(tokens_here, heads_here, key_dim)
-    value_vals = value_rows.astype(jnp.float32).reshape(tokens_here, heads_here, value_dim)
-    new_state = decay[..., None] * carried_state + key_vals[..., None] * value_vals[:, :, None, :]
-    readout = jnp.einsum("bhk,bhkv->bhv", query_scaled, new_state, precision=lax.Precision.HIGHEST)
-    gate_vals = jax.nn.silu(outgate.astype(jnp.float32).reshape(tokens_here, heads_here, value_dim))
-    gated = (readout * rms_factor(readout) * head_gain.astype(jnp.float32) * gate_vals).astype(
-        jnp.bfloat16
+    gated, sel, comb_hi, comb_lo, new_state = run_attention(
+        hidden_in,
+        input_gain[None, :],
+        decay_shift,
+        head_gain.reshape(1, -1),
+        routes,
+        route_weights,
+        query_weight,
+        key_weight,
+        value_weight,
+        outgate_weight,
+        decay_weight,
+        carried_state,
+        lax.axis_size("ep"),
     )
-    gated = gated.reshape(tokens_here, heads_here * value_dim)
-    hid_own = lax.dynamic_slice_in_dim(hidden_in, lane_start, quarter, 1)
-    own_gain = lax.dynamic_slice_in_dim(channel_gain, lane_start, quarter, 0)
-    own_branch = lax.dynamic_slice_in_dim(branch_gate, lane_start, quarter, 0)
-    expert_count = lax.axis_size("ep")
-    topk = routes.shape[1]
-    capacity = tokens_here * topk // expert_count + 2
-    cap = (capacity + 15) // 16 * 16
-    chosen = (
-        routes[:, :, None] == jnp.arange(expert_count, dtype=jnp.int32)[None, None, :]
-    ).astype(jnp.int32)
-    chosen_flat = chosen.reshape(tokens_here * topk, expert_count)
-    index = jnp.arange(tokens_here * topk, dtype=jnp.int32)
-    before = (index[:, None] > index[None, :]).astype(jnp.bfloat16)
-    earlier = matmul(before, chosen_flat.astype(jnp.bfloat16))
-    slot_index = jnp.sum(earlier * chosen_flat, axis=1).astype(jnp.int32)
-    position = routes * cap + slot_index.reshape(tokens_here, topk)
-    slot_table = jnp.arange(expert_count * cap, dtype=jnp.int32)
-    sel = jnp.sum((slot_table[:, None, None] == position[None, :, :]).astype(jnp.float32), axis=2)
-    sel = jnp.pad(sel, ((0, 0), (0, -tokens_here % 128))).astype(jnp.bfloat16)
-    sel = sel.reshape(expert_count, cap, sel.shape[1])
-    comb = jnp.sum(
-        jnp.where(position[:, :, None] == slot_table, route_weights[:, :, None], 0.0), axis=1
-    )
-    comb_hi = lax.optimization_barrier(comb.astype(jnp.bfloat16))
-    comb_lo = (comb - comb_hi.astype(jnp.float32)).astype(jnp.bfloat16)
     mixed = run_layer(
         gated,
         output_weight,
-        hid_own,
-        own_gain.astype(jnp.float32)[None, :],
-        own_branch.astype(jnp.float32)[None, :],
+        hidden_in,
+        channel_gain[None, :],
+        branch_gate[None, :],
         sel,
         comb_hi,
         comb_lo,

time: 81.4 us -> 74.9 us (0.920)
  Pallas kernels: 57.4 us -> 67.3 us
  other arithmetic: 8.66 us -> 0 us
  matrix products: 8.54 us -> 0 us
  local copies, waits for them, and re-layouts: 5.63 us -> 6.65 us
    pallas_call x0 -> x1, Pallas kernels: none -> 9.88 us  [run_attention(): pl.pallas_call(functools.partial(attention_kernel, cap), out_shape=(jax.S...]
    dot_general x7 -> x0, matrix products: 8.54 us -> none  [the longest x6 5.45 us: matmul(): return jnp.dot(left, right, preferred_element_type=jnp.float32)]
    add x2 -> x0, other arithmetic: 4.52 us -> none  [the longest x1 4.52 us: body(): decay[..., None] * carried_state]
    broadcast_in_dim x0 -> x3, local copies, waits for them, and re-layouts: none -> 2.48 us  [the longest x1 1.28 us: body(): input_gain[None, :]]
    convert_element_type x4 -> x0, other arithmetic: 1.39 us -> none  [the longest x1 0.78 us: body(): input_gain.astype(jnp.float32)]
    broadcast_in_dim x1 -> x0, other arithmetic: 1.37 us -> none  [body(): own_branch.astype(jnp.float32)[None, :]]
    reduce_sum x4 -> x0, other arithmetic: 1.36 us -> none  [the longest x2 1.18 us: rms_factor(): jnp.mean(values * values, axis=-1, keepdims=True) + EPSILON]
    unnamed x21 -> x7, local copies, waits for them, and re-layouts: 4.05 us -> 4.17 us
where the time goes in v2:
time: 74.9 us; the launch traced here: 74.6 us
  Pallas kernels  67.3 us (90%)
  local copies, waits for them, and re-layouts  6.65 us (9%)
    pallas_call x1, Pallas kernels, run_layer(): pl.pallas_call(functools.partial(layer_kernel, n_ep, n_tp), out_shape=jax...  57.5 us
    pallas_call x1, Pallas kernels, run_attention(): pl.pallas_call(functools.partial(attention_kernel, cap), out_shape=(jax.S...  9.88 us
    unnamed x7, local copies, waits for them, and re-layouts  4.17 us

profile of v2, /device:TPU:1, one launch (start us, length us, event | category | flops | bytes accessed | tf_op | source)
XLA Modules:
  0.0 74.6 jit_solution(13182014648364790529)
XLA Ops:
  0.6 1.4 %copy.23.routes_ref = s32[48,2]{1,0:T(8,128)} copy(s32[48,2]{0,1:T(2,128)} %param.34) | data formatting | bytes 768 | tf_op args[13]
  2.0 1.4 %copy.24.weights_ref = f32[48,2]{1,0:T(8,128)} copy(f32[48,2]{0,1:T(2,128)} %param.35) | data formatting | bytes 768 | tf_op args[14]
  3.4 1.3 %broadcast_in_dim.9.gain_ref = bf16[1,2048]{1,0:T(2,128)(2,1)} reshape(bf16[2048]{0:T(1024)(128)(2,1)} %param.23) | data formatting | bytes 8192 | tf_op jit(solution)/shard_map/broadcast_in_dim | solution.py:494
  4.7 0.0 copy-start
  4.7 0.0 copy-start.1
  4.7 9.9 %shard_map.212 = (bf16[48,256]{1,0:T(8,128)(2,1)}, bf16[128,128]{1,0:T(8,128)(2,1)}, bf16[48,128]{1,0:T(8,128)(2,1)}, bf16[48,128]{1,0:T(8,128)(2,1)}, f32[48,1,128,256]{3,2,1,0:T(8,128)}) custom-call(bf16[48,2048]{1,0:T(8,128)(2,1)} %hid_ref.1, bf16[1,2048]{1,0:T(2,128)(2,1)} %broadcast_in_dim.9.gain_ref, f32[48,128]{1,0:T(8,128)} %shift_ref.1, ...), custom_call_target="tpu_custom_call" | custom-call | tf_op jit(solution)/shard_map/pallas_call | solution.py:441
  14.5 0.0 copy-done
  14.6 0.6 broadcast_in_dim.10.gain_ref
  15.2 0.0 copy-done.1
  15.2 0.6 broadcast_in_dim.11.gate_ref
  15.8 57.5 %shard_map.213 = bf16[48,512]{1,0:T(8,128)(2,1)} custom-call(bf16[48,256]{1,0:T(8,128)(2,1)} %get-tuple-element.7.gated_ref, bf16[256,2048]{1,0:T(8,128)(2,1)} %outw_ref.1, bf16[48,2048]{1,0:T(8,128)(2,1)} %hid_ref.1, bf16[1,2048]{1,0:T(2,128)(2,1)} %broadcast_in_dim.10.gain_ref, bf16[1,2048]{1,0:T(2,128)(2,1)} %broadcast_in_dim.11.gate_ref, ...), custom_call_target="tpu_custom_call" | custom-call | tf_op jit(solution)/shard_map/pallas_call | solution.py:287
  73.2 1.4 %copy.26 = bf16[48,512]{1,0:T(8,128)(2,1)} copy(bf16[48,512]{1,0:T(8,128)(2,1)} %shard_map.213) | data formatting | bytes 98304
Async XLA Ops:
  4.7 9.9 %copy-start = (bf16[2048]{0:T(1024)(128)(2,1)S(1)}, bf16[2048]{0:T(1024)(128)(2,1)}, u32[]{:S(2)}) copy-start(bf16[2048]{0:T(1024)(128)(2,1)} %param.32) | copy-start | bytes 12292
  4.7 10.5 %copy-start.1 = (bf16[2048]{0:T(1024)(128)(2,1)S(1)}, bf16[2048]{0:T(1024)(128)(2,1)}, u32[]{:S(2)}) copy-start(bf16[2048]{0:T(1024)(128)(2,1)} %param.33) | copy-start | bytes 12292
